TPU v7x, 256 devices: a whole 4x4x8 slice. The times are simulated.
256 devices in a mesh: sp: 64 (over z, y, core), tp: 4 (over x).
Axes of the slice: x: 4, y: 4, z: 8, core: 2. Of those that a mesh axis runs over, the one named last changes fastest.
Arguments:
- b_gate: bfloat16 [32768, 2048], P('sp', 'tp'), may hold values from -6 to 6
- c_gate: bfloat16 [32768, 2048], P('sp', 'tp'), may hold values from -6 to 6
- values_in: bfloat16 [32768, 2048], P('sp', 'tp'), may hold values from -6 to 6
- conv_taps: float32 [3, 2048], P(None, 'tp'), may hold values from -4 to 4
- out_proj: bfloat16 [2048, 2048], P('tp'), may hold values from -0.125 to 0.125
- resid: bfloat16 [32768, 2048], P(('sp', 'tp')), may hold values from -6 to 6
- post_gain: float32 [2048], replicated, may hold values from 0.1 to 1.9
- pre_gain: float32 [2048], replicated, may hold values from 0.1 to 1.9
- moe_gain: float32 [2048], replicated, may hold values from 0.1 to 1.9
- routes: int32 [32768, 4], P(('sp', 'tp')), may hold values from 0 to 63, all different within a row; in each aligned block of 128 rows (0 to 127, 128 to 255, ...) at most 16 rows name the same one
- route_weight: float32 [32768, 4], P(('sp', 'tp')), may hold values from 0.1 to 1
- gate_w: bfloat16 [64, 2048, 640], P('sp'), may hold values from -1 to 1
- up_w: bfloat16 [64, 2048, 640], P('sp'), may hold values from -1 to 1
- down_w: bfloat16 [64, 640, 2048], P('sp'), may hold values from -0.25 to 0.25
Outputs:
- result: bfloat16 [32768, 2048], P(('sp', 'tp'))
Inputs may be any that keep to these rules, and one draw needn't show every extreme that they name: `routes`: each row names 4 different experts; within each aligned block of 128 rows no expert is named by more than 16 rows.
All inputs are finite; a program needn't handle non-finite values.
Results may differ from a plain program's by a relative error of at most 0.007.
Values may be sent and summed in bfloat16 or wider, within the bound.
A program may use at most 64 MiB of HBM per device.

v0:
```python
import jax
import jax.numpy as jnp
from jax import lax
from jax.sharding import PartitionSpec as P

epsilon = 1e-06


def shifted(shard, axis, by):
    devices = lax.axis_size(axis)
    pairs = [(i, i + by) for i in range(devices) if 0 <= i + by < devices]
    return lax.ppermute(shard, axis, pairs)


def in_blocks(shard, dim, devices):
    lengths = shard.shape
    parts = shard.reshape(*lengths[:dim], devices, lengths[dim] // devices, *lengths[dim + 1 :])
    return jnp.moveaxis(parts, dim, 0)


def summed_on_arrival(shard, axis, dim):
    parts = in_blocks(shard, dim, lax.axis_size(axis))
    arrived = lax.all_to_all(parts, axis, split_axis=0, concat_axis=0, tiled=True)
    return arrived.sum(axis=0)


def rms_norm(vector, gain):
    return vector * lax.rsqrt(jnp.mean(vector * vector, axis=-1, keepdims=True) + epsilon) * gain


def body(
    b_gate,
    c_gate,
    values_in,
    conv_taps,
    out_proj,
    resid,
    post_gain,
    pre_gain,
    moe_gain,
    routes,
    route_weight,
    gate_w,
    up_w,
    down_w,
):
    tok_rows = b_gate.shape[0]
    edge_rows = shifted((c_gate[tok_rows - 2 :], values_in[tok_rows - 2 :]), "sp", 1)
    prior_rows = edge_rows[0].astype(jnp.float32) * edge_rows[1].astype(jnp.float32)
    product = c_gate.astype(jnp.float32) * values_in.astype(jnp.float32)
    padded = jnp.concatenate([prior_rows, product], axis=0)
    filtered = (
        padded[0:tok_rows] * conv_taps[0]
        + padded[1 : tok_rows + 1] * conv_taps[1]
        + padded[2 : tok_rows + 2] * conv_taps[2]
    )
    mixed_rows = (b_gate.astype(jnp.float32) * filtered).astype(jnp.bfloat16)
    projected = summed_on_arrival(
        jnp.dot(mixed_rows, out_proj, preferred_element_type=jnp.float32), "tp", 0
    )
    stream = (resid.astype(jnp.float32) + rms_norm(projected, post_gain)).astype(jnp.bfloat16)
    normed = rms_norm(stream.astype(jnp.float32), pre_gain).astype(jnp.bfloat16)
    own_count = normed.shape[0]
    width = normed.shape[1]
    top_count = routes.shape[1]
    experts = lax.axis_size("sp")
    capacity = 2 * own_count * top_count // experts
    flat_ids = routes.reshape(-1)
    assigned = flat_ids.shape[0]
    onehot = (flat_ids[:, None] == jnp.arange(experts, dtype=jnp.int32)[None, :]).astype(jnp.int32)
    earlier = jnp.cumsum(onehot, axis=0) - onehot
    slot_index = jnp.sum(earlier * onehot, axis=1)
    target = flat_ids * capacity + slot_index
    source = (
        jnp.full((experts * capacity,), assigned, jnp.int32)
        .at[target]
        .set(jnp.arange(assigned, dtype=jnp.int32))
    )
    row_index = jnp.where(source < assigned, source // top_count, own_count)
    with_blank = jnp.concatenate([normed, jnp.zeros((1, width), jnp.bfloat16)], axis=0)
    outgoing = with_blank[row_index].reshape(experts, capacity, width)
    slots_in = lax.all_to_all(outgoing, "sp", split_axis=0, concat_axis=0, tiled=True)
    gate_pre = jnp.dot(slots_in, gate_w[0], preferred_element_type=jnp.float32)
    up_pre = jnp.dot(slots_in, up_w[0], preferred_element_type=jnp.float32)
    gate_act = jnp.minimum(gate_pre, 7.0)
    up_act = jnp.clip(up_pre, -7.0, 7.0)
    hidden = (gate_act * jax.nn.sigmoid(1.702 * gate_act) * (up_act + 1.0)).astype(jnp.bfloat16)
    expert_out = jnp.dot(hidden, down_w[0], preferred_element_type=jnp.float32).astype(jnp.bfloat16)
    returned = lax.all_to_all(expert_out, "sp", split_axis=0, concat_axis=0, tiled=True)
    chosen = returned.reshape(experts * capacity, width)[target].astype(jnp.float32)
    weighted = chosen * route_weight.reshape(-1)[:, None]
    combined = jnp.sum(weighted.reshape(own_count, top_count, width), axis=1)
    return (stream.astype(jnp.float32) + rms_norm(combined, moe_gain)).astype(jnp.bfloat16)


def solution(mesh):
    placed = (
        P("sp", "tp"),
        P("sp", "tp"),
        P("sp", "tp"),
        P(None, "tp"),
        P("tp", None),
        P(("sp", "tp"), None),
        P(),
        P(),
        P(),
        P(("sp", "tp"), None),
        P(("sp", "tp"), None),
        P("sp", None, None),
        P("sp", None, None),
        P("sp", None, None),
    )
    return jax.shard_map(
        body, mesh=mesh, in_specs=placed, out_specs=P(("sp", "tp"), None), check_vma=False
    )
```

profile of v0, /device:TPU:1, one launch (start us, length us, event | category | flops | bytes accessed | tf_op | source)
XLA Modules:
  0.0 330.8 jit_solution(4011597702440219047)
XLA Ops:
  0.0 0.9 slice.27
  0.9 4.6 %collective-permute-start = (bf16[2,512]{1,0:T(2,128)(2,1)S(1)}, bf16[2,512]{1,0:T(2,128)(2,1)S(1)}, u32[]{:S(2)}, u32[]{:S(2)}) collective-permute-start(bf16[2,512]{1,0:T(2,128)(2,1)S(1)} %slice.27), channel_id=1, source_target_pairs={{0,4},{4,8},{8,12},{12,16},{16,20},{20,24},{24,28},{28,32},{32,36}... | collective-permute-start | bytes 6152 | tf_op jit(solution)/shard_map/ppermute | solution.py:12
  5.4 0.7 slice.28
  6.1 1.9 collective-permute-start.1
  8.1 1.3 convert_multiply_fusion.2
  9.4 0.8 fusion.40
  10.3 5.2 %fusion.20 = f32[512,2048]{1,0:T(8,128)} fusion(bf16[512,2048]{1,0:T(8,128)(2,1)} %param.18, f32[2,512]{1,0:T(2,128)S(1)} %convert_multiply_fusion.3, f32[512,512]{1,0:T(8,128)S(1)} %convert_multiply_fusion.2, bf16[512,512]{1,0:T(8,128)(2,1)} %param.14, f32[512]{0:T(512)S(1)} %bitcast.49, f32[512]{0:T(512)S(1)} %bitcast.50, f32[512]{0:T(512)S(1)} %bitcast.48), kind=kOutput, calls=%fused_computation.32 | convolution fusion | flops 1076363264 | bytes 7874560 | tf_op jit(solution)/shard_map/dot_general | solution.py:59
  15.4 5.0 %all-to-all-start = ((f32[4,128,2048]{2,1,0:T(8,128)}), f32[4,128,2048]{2,1,0:T(8,128)}, u32[]{:S(2)}, u32[]{:S(2)}) async-start(f32[4,128,2048]{2,1,0:T(8,128)} %bitcast.47), calls=%async_computation | async-start | bytes 8388608 | tf_op jit(solution)/shard_map/all_to_all | solution.py:23
  20.4 0.1 copy.17
  20.8 1.2 reduce-window.6
  22.0 0.2 slice_reduce_fusion
  22.3 0.1 copy.16
  22.5 0.1 fusion.27
  22.6 2.4 scatter_custom_fusion
  25.1 43.7 %all-to-all-done = f32[4,128,2048]{2,1,0:T(8,128)} async-done(((f32[4,128,2048]{2,1,0:T(8,128)}), f32[4,128,2048]{2,1,0:T(8,128)}, u32[]{:S(2)}, u32[]{:S(2)}) %all-to-all-start) | async-done | bytes 4194336 | tf_op jit(solution)/shard_map/all_to_all | solution.py:23
  68.9 3.6 %reduce_sum.56 = f32[128,2048]{1,0:T(8,128)} reduce(f32[4,128,2048]{2,1,0:T(8,128)} %all-to-all-done, f32[]{:T(128)} %constant.18.clone.1), dimensions={0}, to_apply=%region_0.0 | reduce | flops 786432 | bytes 5242884 | tf_op jit(solution)/shard_map/reduce_sum | solution.py:24
  72.5 1.4 multiply_reduce_fusion.2
  73.9 1.6 fusion.13
  75.5 0.8 copy-done.1
  76.3 0.2 fusion.15
  76.5 6.0 %gather_fusion = bf16[1024,2048]{1,0:T(8,128)(2,1)} fusion(bf16[129,2048]{1,0:T(8,128)(2,1)S(1)} %concatenate.7, s32[1024]{0:T(1024)S(1)} %fusion.31), kind=kCustom, calls=%fused_computation | custom fusion | bytes 8392704 | tf_op jit(solution)/shard_map/gather | solution.py:81
  82.5 107.5 %all_to_all.15 = bf16[64,16,2048]{2,1,0:T(8,128)(2,1)S(1)} all-to-all(bf16[64,16,2048]{2,1,0:T(8,128)(2,1)} %bitcast.46), channel_id=1, replica_groups=mesh['sp'=64,'tp'=4] {'sp'}, dimensions={0} | all-to-all | bytes 8388608 | tf_op jit(solution)/shard_map/all_to_all | solution.py:82
  190.0 2.0 copy-done.3
  192.0 5.0 %fusion.1 = f32[64,16,640]{2,1,0:T(8,128)} fusion(bf16[64,16,2048]{2,1,0:T(8,128)(2,1)S(1)} %all_to_all.15, bf16[1,2048,640]{2,1,0:T(8,128)(2,1)S(1)} %copy-done.10), kind=kOutput, calls=%fused_computation.6 | convolution fusion | flops 2684354560 | bytes 9437184 | tf_op jit(solution)/shard_map/dot_general | solution.py:84
  197.0 12.1 %convolution_convert_fusion = bf16[64,16,2048]{2,1,0:T(8,128)(2,1)} fusion(bf16[1,640,2048]{2,1,0:T(8,128)(2,1)S(1)} %copy-done, f32[64,16,640]{2,1,0:T(8,128)} %fusion.1, bf16[64,16,2048]{2,1,0:T(8,128)(2,1)} %copy-done.3, bf16[1,2048,640]{2,1,0:T(8,128)(2,1)} %param.25), kind=kOutput, calls=%fused_computation.4 | convolution fusion | flops 5377359872 | bytes 16252928 | tf_op jit(solution)/shard_map/dot_general | solution.py:88
  209.1 7.4 %all-to-all-start.2 = ((bf16[64,16,2048]{2,1,0:T(8,128)(2,1)}), bf16[64,16,2048]{2,1,0:T(8,128)(2,1)}, u32[]{:S(2)}, u32[]{:S(2)}) async-start(bf16[64,16,2048]{2,1,0:T(8,128)(2,1)} %convolution_convert_fusion), calls=%async_computation.2 | async-start | bytes 8388608 | tf_op jit(solution)/shard_map/all_to_all | solution.py:89
  216.6 94.8 %all-to-all-done.2 = bf16[64,16,2048]{2,1,0:T(8,128)(2,1)} async-done(((bf16[64,16,2048]{2,1,0:T(8,128)(2,1)}), bf16[64,16,2048]{2,1,0:T(8,128)(2,1)}, u32[]{:S(2)}, u32[]{:S(2)}) %all-to-all-start.2) | async-done | bytes 4194336 | tf_op jit(solution)/shard_map/all_to_all | solution.py:89
  311.4 8.0 %gather_fusion.1 = bf16[512,2048]{1,0:T(8,128)(2,1)} fusion(bf16[1024,2048]{1,0:T(8,128)(2,1)} %bitcast.14, s32[1024]{0:T(1024)S(1)} %pad_clamp_fusion), kind=kCustom, calls=%fused_computation.1 | custom fusion | bytes 4196352 | tf_op jit(solution)/shard_map/gather | solution.py:90
  319.4 4.8 %reshape.96 = f32[128,4,2048]{2,1,0:T(4,128)} reshape(bf16[512,2048]{1,0:T(8,128)(2,1)} %gather_fusion.1) | data formatting | bytes 6291456 | tf_op jit(solution)/shard_map/convert_element_type | solution.py:90
  324.1 5.5 %multiply_reduce_fusion = f32[128,2048]{1,0:T(8,128)S(1)} fusion(f32[128,4,2048]{2,1,0:T(4,128)} %reshape.96, f32[128,4]{1,0:T(8,128)S(1)} %copy.20), kind=kLoop, calls=%fused_computation.3 | loop fusion | flops 1835008 | bytes 5244928 | tf_op jit(solution)/shard_map/reduce_sum | solution.py:92
  329.6 0.2 multiply_reduce_fusion.1
  329.8 1.0 fusion.16
  (39 shorter events, 0.6 us)
Async XLA Ops:
  0.0 197.0 %copy-start = (bf16[1,640,2048]{2,1,0:T(8,128)(2,1)S(1)}, bf16[1,640,2048]{2,1,0:T(8,128)(2,1)}, u32[]{:S(2)}) copy-start(bf16[1,640,2048]{2,1,0:T(8,128)(2,1)} %param.27) | copy-start | bytes 7864324
  0.9 9.4 %collective-permute-start = (bf16[2,512]{1,0:T(2,128)(2,1)S(1)}, bf16[2,512]{1,0:T(2,128)(2,1)S(1)}, u32[]{:S(2)}, u32[]{:S(2)}) collective-permute-start(bf16[2,512]{1,0:T(2,128)(2,1)S(1)} %slice.27), channel_id=1, source_target_pairs={{0,4},{4,8},{8,12},{12,16},{16,20},{20,24},{24,28},{28,32},{32,36}... | collective-permute-start | bytes 6152 | tf_op jit(solution)/shard_map/ppermute | solution.py:12
  6.1 4.1 %collective-permute-start.1 = (bf16[2,512]{1,0:T(2,128)(2,1)S(1)}, bf16[2,512]{1,0:T(2,128)(2,1)S(1)}, u32[]{:S(2)}, u32[]{:S(2)}) collective-permute-start(bf16[2,512]{1,0:T(2,128)(2,1)S(1)} %slice.28), channel_id=1, source_target_pairs={{0,4},{4,8},{8,12},{12,16},{16,20},{20,24},{24,28},{28,32},{32,36}... | collective-permute-start | bytes 6152 | tf_op jit(solution)/shard_map/ppermute | solution.py:12
  15.4 5.0 %copy-start.8 = (s32[128,4]{0,1:T(4,128)S(1)}, s32[128,4]{0,1:T(4,128)}, u32[]{:S(2)}) copy-start(s32[128,4]{0,1:T(4,128)} %param.23) | copy-start | bytes 6148
  15.4 53.5 %all-to-all-start = ((f32[4,128,2048]{2,1,0:T(8,128)}), f32[4,128,2048]{2,1,0:T(8,128)}, u32[]{:S(2)}, u32[]{:S(2)}) async-start(f32[4,128,2048]{2,1,0:T(8,128)} %bitcast.47), calls=%async_computation | async-start | bytes 8388608 | tf_op jit(solution)/shard_map/all_to_all | solution.py:23
  25.1 48.8 %copy-start.4 = (bf16[128,2048]{1,0:T(8,128)(2,1)S(1)}, bf16[128,2048]{1,0:T(8,128)(2,1)}, u32[]{:S(2)}) copy-start(bf16[128,2048]{1,0:T(8,128)(2,1)} %param.19) | copy-start | bytes 1572868
  25.1 48.7 %copy-start.5 = (f32[2048]{0:T(1024)S(1)}, f32[2048]{0:T(1024)}, u32[]{:S(2)}) copy-start(f32[2048]{0:T(1024)} %param.20) | copy-start | bytes 24580
  72.5 3.8 %copy-start.6 = (f32[2048]{0:T(1024)S(1)}, f32[2048]{0:T(1024)}, u32[]{:S(2)}) copy-start(f32[2048]{0:T(1024)} %param.21) | copy-start | bytes 24580
  75.5 0.8 copy-start.1
  82.5 109.5 %copy-start.10 = (bf16[1,2048,640]{2,1,0:T(8,128)(2,1)S(1)}, bf16[1,2048,640]{2,1,0:T(8,128)(2,1)}, u32[]{:S(2)}) copy-start(bf16[1,2048,640]{2,1,0:T(8,128)(2,1)} %param.26) | copy-start | bytes 7864324
  190.0 2.0 copy-start.3
  209.1 7.4 %copy-start.9 = (f32[128,4]{0,1:T(4,128)S(1)}, f32[128,4]{0,1:T(4,128)}, u32[]{:S(2)}) copy-start(f32[128,4]{0,1:T(4,128)} %param.24) | copy-start | bytes 6148
  209.1 102.3 %all-to-all-start.2 = ((bf16[64,16,2048]{2,1,0:T(8,128)(2,1)}), bf16[64,16,2048]{2,1,0:T(8,128)(2,1)}, u32[]{:S(2)}, u32[]{:S(2)}) async-start(bf16[64,16,2048]{2,1,0:T(8,128)(2,1)} %convolution_convert_fusion), calls=%async_computation.2 | async-start | bytes 8388608 | tf_op jit(solution)/shard_map/all_to_all | solution.py:89
  324.1 5.6 %copy-start.2 = (bf16[128,2048]{1,0:T(8,128)(2,1)S(1)}, bf16[128,2048]{1,0:T(8,128)(2,1)}, u32[]{:S(2)}) copy-start(bf16[128,2048]{1,0:T(8,128)(2,1)} %copy-done.1) | copy-start | bytes 1572868
  324.1 5.7 %copy-start.7 = (f32[2048]{0:T(1024)S(1)}, f32[2048]{0:T(1024)}, u32[]{:S(2)}) copy-start(f32[2048]{0:T(1024)} %param.22) | copy-start | bytes 24580
where the time goes:
time: 332 us; the launch traced here: 331 us
  waiting for transfers between devices  139 us (42%)
  blocking collectives  107 us (32%)
  local copies, waits for them, and re-layouts  27.3 us (8%)
  matrix products  22.2 us (7%)
  starting transfers between devices  18.9 us (6%)
  other arithmetic  16.2 us (5%)
    all_to_all x1, blocking collectives, body(): lax.all_to_all(outgoing, 'sp', split_axis=0, concat_axis=0, tiled=True)  107 us
    all_to_all x1, waiting for transfers between devices, body(): lax.all_to_all(expert_out, 'sp', split_axis=0, concat_axis=0, tiled=True)  94.8 us
    all_to_all x1, waiting for transfers between devices, summed_on_arrival(): lax.all_to_all(parts, axis, split_axis=0, concat_axis=0, tiled=True)  43.7 us
    dot_general x1, matrix products, body(): jnp.dot(hidden, down_w[0], preferred_element_type=jnp.float32)  12.1 us
    gather x1, local copies, waits for them, and re-layouts, body(): returned.reshape(experts * capacity, width)[target].astype(jnp.float32)  7.96 us
    all_to_all x1, starting transfers between devices, body(): lax.all_to_all(expert_out, 'sp', split_axis=0, concat_axis=0, tiled=True)  7.42 us
  transfers between devices with their start and end apart: 4, of which 2 were waited for; matrix products, arithmetic and copies ran while one was open for 2% of the time, Pallas kernels for 0%

commit v1 on v0

v1 whole, which is shorter than its diff:
```python
import jax
import jax.numpy as jnp
from jax import lax
from jax.experimental import pallas as pl
from jax.experimental.pallas import tpu as pltpu
from jax.sharding import PartitionSpec as P

EPS = 1e-06
F32 = jnp.float32
BF16 = jnp.bfloat16
MESH = pl.DeviceIdType.MESH
D = 2048
FF = 640
ROWS = 128
CAP = 16
HALF = ROWS // 2
COLS = 512
SOURCE_OF = (0, -1, 1, -2, 2, -3, 3, 4)
STEPS = ((0, 1), (1, 2), (3, 2), (5, 2), (7, 1))
MOVES = ((2, 0), (1, 0), (3, 0), (2, 1), (1, 1), (3, 1), (0, 1))


def rows_loop(count, size, fn):
    def step(i, carry):
        fn(pl.ds(pl.multiple_of(i * size, size), size))
        return carry

    lax.fori_loop(0, count, step, 0)


def kernel(
    b_ref, c_ref, v_ref, taps_ref, wproj_ref, resid_ref, post_ref, pre_ref, moe_ref, rw_ref,
    gw_ref, uw_ref, dw_ref,
    out_ref,
    wgu, dwv, edge, prodp, mixed, p0, p1, p3, x2, s1, s3, ra, rb, fm, fp,
    stream, xs, rwall, pmat, wmat, sel, rin, hid, eout, rback, part_u, part_d, su, sd, ru, rd,
    w_sem, e_ss, e_rs, rw_ss, rw_rs, x_ss, x_rs, ag_ss, ag_rs, d_ss, d_rs, r_ss, r_rs, z_ss, z_rs,
):
    sp = lax.axis_index("sp")
    tp = lax.axis_index("tp")
    z = sp // 8
    k = lax.rem(sp, 8)
    y = k // 2
    c = lax.rem(k, 2)

    def zdev(by):
        return {"sp": lax.rem(z + by + 8, 8) * 8 + k, "tp": tp}

    def in_plane(dy, dc):
        other = 1 - c if dc else c
        return lax.rem(y + dy + 4, 4) * 2 + other

    def pdev(index):
        return {"sp": z * 8 + index, "tp": tp}

    def xdev(by):
        return {"sp": sp, "tp": lax.rem(tp + by + 4, 4)}

    def sdev(by):
        return {"sp": lax.rem(sp + by + 64, 64), "tp": tp}

    def rcopy(src, dst, ss, rs, dev):
        return pltpu.make_async_remote_copy(
            src_ref=src, dst_ref=dst, send_sem=ss, recv_sem=rs, device_id=dev, device_id_type=MESH
        )

    weights = []
    for n in range(5):
        cols = pl.ds(n * 128, 128)
        weights.append(pltpu.make_async_copy(gw_ref.at[0, :, cols], wgu.at[n, :, pl.ds(0, 128)], w_sem.at[2 * n]))
        weights.append(pltpu.make_async_copy(uw_ref.at[0, :, cols], wgu.at[n, :, pl.ds(128, 128)], w_sem.at[2 * n + 1]))
    weights.append(pltpu.make_async_copy(dw_ref.at[0], dwv, w_sem.at[10]))
    for w in weights:
        w.start()

    barrier = pltpu.get_barrier_semaphore()
    peers = [xdev(1), xdev(2), xdev(3), sdev(1), sdev(-1)]
    peers += [zdev(by) for by in range(1, 8)]
    peers += [pdev(in_plane(dy, dc)) for dy, dc in MOVES]
    for dev in peers:
        pl.semaphore_signal(barrier, inc=1, device_id=dev, device_id_type=MESH)
    pl.semaphore_wait(barrier, len(peers))

    last = pl.ds(b_ref.shape[0] - 16, 16)
    edges = [
        rcopy(c_ref.at[last], edge.at[0], e_ss.at[0], e_rs.at[0], sdev(1)),
        rcopy(v_ref.at[last], edge.at[1], e_ss.at[1], e_rs.at[1], sdev(1)),
    ]
    for e in edges:
        e.start()
    routing = [
        rcopy(rw_ref, rwall.at[i], rw_ss.at[i], rw_rs.at[i], zdev(-SOURCE_OF[i])) for i in range(1, 8)
    ]
    for r in routing:
        r.start()
    rwall[0] = rw_ref[...]

    for i in range(4):
        rows = pl.ds(i * ROWS, ROWS)
        prodp[pl.ds(16 + i * ROWS, ROWS), :] = c_ref[rows, :].astype(F32) * v_ref[rows, :].astype(F32)
    for e in edges:
        e.wait_recv()
    prior = edge[0].astype(F32) * edge[1].astype(F32)
    prodp[0:16, :] = jnp.where(sp > 0, prior, jnp.zeros_like(prior))
    for i in range(4):
        at = i * ROWS
        filtered = (
            prodp[at + 14 : at + 14 + ROWS, :] * taps_ref[0:1, :]
            + prodp[at + 15 : at + 15 + ROWS, :] * taps_ref[1:2, :]
            + prodp[at + 16 : at + 16 + ROWS, :] * taps_ref[2:3, :]
        )
        mixed[at : at + ROWS, :] = (b_ref[at : at + ROWS, :].astype(F32) * filtered).astype(BF16)

    def project(by, dst):
        block = pl.ds(pl.multiple_of(lax.rem(tp + by, 4) * ROWS, ROWS), ROWS)

        def cols(at):
            got = jnp.dot(mixed[block, :], wproj_ref[:, at], preferred_element_type=F32)
            dst[:, at] = got.astype(dst.dtype)

        rows_loop(D // COLS, COLS, cols)

    lo, hi = pl.ds(0, HALF), pl.ds(HALF, HALF)

    project(2, x2)
    far_a = rcopy(x2.at[lo], ra, x_ss.at[0], x_rs.at[0], xdev(1))
    far_b = rcopy(x2.at[hi], rb, x_ss.at[1], x_rs.at[1], xdev(-1))
    far_a.start()
    far_b.start()
    project(1, p1)
    project(3, p3)

    def cast_rows(src, dst, base):
        def rows(at):
            dst[at, :] = src[at, :].astype(BF16)

        def step(i, carry):
            rows(pl.ds(pl.multiple_of(base + i * 16, 16), 16))
            return carry

        lax.fori_loop(0, HALF // 16, step, 0)

    def add_rows(src, more, shift, dst, base):
        def step(i, carry):
            at = pl.ds(pl.multiple_of(base + i * 16, 16), 16)
            there = pl.ds(pl.multiple_of(base - shift + i * 16, 16), 16)
            dst[at, :] = (src[at, :] + more[there, :].astype(F32)).astype(BF16)
            return carry

        lax.fori_loop(0, HALF // 16, step, 0)

    cast_rows(p1, s1, HALF)
    near_1b = rcopy(s1.at[hi], fm.at[hi], x_ss.at[2], x_rs.at[2], xdev(1))
    near_1b.start()
    cast_rows(p3, s3, 0)
    near_3a = rcopy(s3.at[lo], fp.at[lo], x_ss.at[3], x_rs.at[3], xdev(-1))
    near_3a.start()
    far_a.wait_recv()
    add_rows(p1, ra, 0, s1, 0)
    near_1a = rcopy(s1.at[lo], fm.at[lo], x_ss.at[4], x_rs.at[4], xdev(1))
    near_1a.start()
    far_b.wait_recv()
    add_rows(p3, rb, HALF, s3, HALF)
    near_3b = rcopy(s3.at[hi], fp.at[hi], x_ss.at[5], x_rs.at[5], xdev(-1))
    near_3b.start()
    project(0, p0)

    for r in routing:
        r.wait_recv()

    def tables(i, carry):
        rw = rwall[i]
        row = lax.broadcasted_iota(jnp.int32, (ROWS, ROWS), 0)
        lane = lax.broadcasted_iota(jnp.int32, (ROWS, ROWS), 1)
        expert = (z * 8 + row // CAP).astype(F32)
        slot = lax.rem(row, CAP).astype(F32)
        named = jnp.zeros((ROWS, ROWS), F32)
        weight = jnp.zeros((ROWS, ROWS), F32)
        for j in range(4):
            hit = rw[j : j + 1, :] == expert
            named = named + jnp.where(hit, 1.0, 0.0)
            weight = weight + jnp.where(hit, jnp.broadcast_to(rw[4 + j : 5 + j, :], (ROWS, ROWS)), 0.0)
        before = jnp.where(row < lane, 1.0, 0.0).astype(BF16)
        earlier = jnp.dot(named.astype(BF16), before, preferred_element_type=F32)
        picked = jnp.where(earlier == slot, named, 0.0)
        pmat[i] = picked.astype(BF16)
        wt = jnp.transpose(picked * weight)
        high = wt.astype(BF16)
        wmat[i, :, 0:ROWS] = high
        wmat[i, :, ROWS : 2 * ROWS] = (wt - high.astype(F32)).astype(BF16)
        return carry

    lax.fori_loop(0, 8, tables, 0)

    near_1b.wait_recv()
    near_1a.wait_recv()
    near_3a.wait_recv()
    near_3b.wait_recv()

    def norms(at):
        proj = p0[at, :] + fm[at, :].astype(F32) + fp[at, :].astype(F32)
        inv = lax.rsqrt(jnp.mean(proj * proj, axis=-1, keepdims=True) + EPS)
        st = (resid_ref[at, :].astype(F32) + proj * inv * post_ref[...]).astype(BF16)
        stream[at, :] = st
        wide = st.astype(F32)
        inv2 = lax.rsqrt(jnp.mean(wide * wide, axis=-1, keepdims=True) + EPS)
        xs[0, at, :] = (wide * inv2 * pre_ref[...]).astype(BF16)

    def ag(step, half, up):
        rows = lo if half == 0 else hi
        src = (0, 1, 3, 5) if up else (0, 2, 4, 6)
        dst = (1, 3, 5, 7) if up else (2, 4, 6, 7)
        at = (0 if up else 8) + 2 * step + half
        return rcopy(
            xs.at[src[step], rows], xs.at[dst[step], rows], ag_ss.at[at], ag_rs.at[at], zdev(1 if up else -1)
        )

    ring = {(s, h, u): ag(s, h, u) for s in range(3) for h in range(2) for u in (True, False)}
    ring[(3, 0, True)] = ag(3, 0, True)
    ring[(3, 1, False)] = ag(3, 1, False)

    for h in range(2):
        def half_rows(i, carry, h=h):
            norms(pl.ds(pl.multiple_of(h * HALF + i * 16, 16), 16))
            return carry

        lax.fori_loop(0, HALF // 16, half_rows, 0)
        ring[(0, h, True)].start()
        ring[(0, h, False)].start()

    def select(i):
        def cols(at):
            got = jnp.dot(pmat[i], xs[i, :, at], preferred_element_type=F32)
            sel[i, :, :, at] = got.astype(BF16).reshape(8, CAP, COLS)

        rows_loop(D // COLS, COLS, cols)

    def plane_sends(si, src, dst, ss, rs):
        first, n = STEPS[si]
        sends, waits = [], []
        for m, (dy, dc) in enumerate(MOVES):
            to = in_plane(dy, dc)
            frm = in_plane(-dy, dc)
            blocks = pl.ds(first, n)
            sends.append(rcopy(src.at[blocks, to], dst.at[blocks, k], ss.at[si, m], rs.at[si, m], pdev(to)))
            waits.append(rcopy(src.at[blocks, frm], dst.at[blocks, frm], ss.at[si, m], rs.at[si, m], pdev(to)))
        return sends, waits

    out_sends = [plane_sends(si, sel, rin, d_ss, d_rs) for si in range(5)]
    back_sends = [plane_sends(si, eout, rback, r_ss, r_rs) for si in range(5)]

    def dispatch(si):
        first, n = STEPS[si]
        for i in range(first, first + n):
            select(i)
        for s in out_sends[si][0]:
            s.start()
        for i in range(first, first + n):
            rin[i, k] = sel[i, k]

    def experts(si):
        first, n = STEPS[si]
        for w in out_sends[si][1]:
            w.wait_recv()
        if si == 0:
            for w in weights:
                w.wait()
        m = n * ROWS

        def gate_up(j, carry):
            x = rin[pl.ds(first, n)].reshape(m, D)
            gu = jnp.dot(x, wgu[j], preferred_element_type=F32)
            gate = jnp.minimum(gu[:, 0:128], 7.0)
            up = jnp.clip(gu[:, 128:256], -7.0, 7.0)
            hid[j, 0:m, :] = (gate * jax.nn.sigmoid(1.702 * gate) * (up + 1.0)).astype(BF16)
            return carry

        lax.fori_loop(0, 5, gate_up, 0)

        def down(at):
            h = jnp.concatenate([hid[j, 0:m, :] for j in range(5)], axis=1)
            got = jnp.dot(h, dwv[:, at], preferred_element_type=F32)
            eout[pl.ds(first, n), :, :, at] = got.astype(BF16).reshape(n, 8, CAP, COLS)

        rows_loop(D // COLS, COLS, down)

    dispatch(0)
    for s in range(1, 4):
        up_step, last_step = s - 1, s == 3
        for h in range(2):
            for u in (True, False):
                ring[(up_step, h, u)].wait_recv()
                if (s, h, u) in ring:
                    ring[(s, h, u)].start()
            if h == 0 and s >= 2:
                experts(s - 2)
        dispatch(s)
    experts(2)
    ring[(3, 0, True)].wait_recv()
    ring[(3, 1, False)].wait_recv()
    dispatch(4)
    experts(3)
    experts(4)

    for si in (4, 3, 2, 1, 0):
        first, n = STEPS[si]
        for s in back_sends[si][0]:
            s.start()
        for i in range(first, first + n):
            rback[i, k] = eout[i, k]

    def combine(i, dst):
        def cols(at):
            r = rback[i, :, :, at].reshape(ROWS, COLS)
            got = jnp.dot(wmat[i, :, 0:ROWS], r, preferred_element_type=F32)
            got = got + jnp.dot(wmat[i, :, ROWS : 2 * ROWS], r, preferred_element_type=F32)
            dst[:, at] = got.astype(dst.dtype)

        rows_loop(D // COLS, COLS, cols)

    def zsend(r, half, up):
        rows = lo if half == 0 else hi
        at = (0 if up else 8) + 2 * r + half
        src, dst = (su, ru) if up else (sd, rd)
        return rcopy(src.at[r, rows], dst.at[r, rows], z_ss.at[at], z_rs.at[at], zdev(1 if up else -1))

    back = {(r, h, u): zsend(r, h, u) for r in range(1, 4) for h in range(2) for u in (True, False)}
    back[(0, 0, True)] = zsend(0, 0, True)
    back[(0, 1, False)] = zsend(0, 1, False)

    for w in back_sends[4][1]:
        w.wait_recv()
    combine(7, part_u)
    cast_rows(part_u, su.at[0], 0)
    back[(0, 0, True)].start()
    cast_rows(part_u, sd.at[0], HALF)
    back[(0, 1, False)].start()
    for r, si in ((1, 3), (2, 2), (3, 1)):
        first, n = STEPS[si]
        for w in back_sends[si][1]:
            w.wait_recv()
        combine(first + 1, part_u)
        combine(first, part_d)
        for h, u in ((1, True), (0, False), (0, True), (1, False)):
            src, send, got = (part_u, su, ru) if u else (part_d, sd, rd)
            if (r - 1, h, u) in back:
                back[(r - 1, h, u)].wait_recv()
                add_rows(src, got.at[r - 1], 0, send.at[r], h * HALF)
            else:
                cast_rows(src, send.at[r], h * HALF)
            back[(r, h, u)].start()

    for w in back_sends[0][1]:
        w.wait_recv()
    combine(0, part_u)
    for h, u in ((1, True), (0, False), (0, True), (1, False)):
        back[(3, h, u)].wait_recv()

    def finish(at):
        total = part_u[at, :] + ru[3, at, :].astype(F32) + rd[3, at, :].astype(F32)
        inv = lax.rsqrt(jnp.mean(total * total, axis=-1, keepdims=True) + EPS)
        out_ref[at, :] = (stream[at, :].astype(F32) + total * inv * moe_ref[...]).astype(BF16)

    rows_loop(ROWS // 16, 16, finish)

    for s in edges + routing + [far_a, far_b, near_1a, near_1b, near_3a, near_3b]:
        s.wait_send()
    for s in list(ring.values()) + list(back.values()):
        s.wait_send()
    for sends, _ in out_sends + back_sends:
        for s in sends:
            s.wait_send()


def body(
    b_gate, c_gate, values_in, conv_taps, out_proj, resid, post_gain, pre_gain, moe_gain,
    routes, route_weight, gate_w, up_w, down_w,
):
    rw = jnp.concatenate([routes.astype(F32), route_weight], axis=1).T
    vmem = pl.BlockSpec(memory_space=pltpu.VMEM)
    hbm = pl.BlockSpec(memory_space=pl.ANY)
    dma = pltpu.SemaphoreType.DMA
    block = (ROWS, D)
    return pl.pallas_call(
        kernel,
        out_shape=jax.ShapeDtypeStruct(block, BF16),
        in_specs=[vmem] * 10 + [hbm] * 3,
        out_specs=vmem,
        scratch_shapes=[
            pltpu.VMEM((5, D, 256), BF16),
            pltpu.VMEM((FF, D), BF16),
            pltpu.VMEM((2, 16, 512), BF16),
            pltpu.VMEM((528, 512), F32),
            pltpu.VMEM((512, 512), BF16),
            pltpu.VMEM(block, F32),
            pltpu.VMEM(block, F32),
            pltpu.VMEM(block, F32),
            pltpu.VMEM(block, BF16),
            pltpu.VMEM(block, BF16),
            pltpu.VMEM(block, BF16),
            pltpu.VMEM((HALF, D), BF16),
            pltpu.VMEM((HALF, D), BF16),
            pltpu.VMEM(block, BF16),
            pltpu.VMEM(block, BF16),
            pltpu.VMEM(block, BF16),
            pltpu.VMEM((8,) + block, BF16),
            pltpu.VMEM((8, 8, 128), F32),
            pltpu.VMEM((8, ROWS, ROWS), BF16),
            pltpu.VMEM((8, ROWS, 2 * ROWS), BF16),
            pltpu.VMEM((8, 8, CAP, D), BF16),
            pltpu.VMEM((8, 8, CAP, D), BF16),
            pltpu.VMEM((5, 2 * ROWS, 128), BF16),
            pltpu.VMEM((8, 8, CAP, D), BF16),
            pltpu.VMEM((8, 8, CAP, D), BF16),
            pltpu.VMEM(block, F32),
            pltpu.VMEM(block, F32),
            pltpu.VMEM((4,) + block, BF16),
            pltpu.VMEM((4,) + block, BF16),
            pltpu.VMEM((4,) + block, BF16),
            pltpu.VMEM((4,) + block, BF16),
            dma((11,)),
            dma((2,)), dma((2,)),
            dma((8,)), dma((8,)),
            dma((6,)), dma((6,)),
            dma((16,)), dma((16,)),
            dma((5, 7)), dma((5, 7)),
            dma((5, 7)), dma((5, 7)),
            dma((16,)), dma((16,)),
        ],
        compiler_params=pltpu.CompilerParams(
            collective_id=0, has_side_effects=True, vmem_limit_bytes=63 * 2**20
        ),
    )(
        b_gate, c_gate, values_in, conv_taps, out_proj, resid,
        post_gain.reshape(1, D), pre_gain.reshape(1, D), moe_gain.reshape(1, D), rw,
        gate_w, up_w, down_w,
    )


def solution(mesh):
    rows = P(("sp", "tp"), None)
    placed = (
        P("sp", "tp"), P("sp", "tp"), P("sp", "tp"), P(None, "tp"), P("tp", None), rows,
        P(), P(), P(), rows, rows,
        P("sp", None, None), P("sp", None, None), P("sp", None, None),
    )
    return jax.shard_map(body, mesh=mesh, in_specs=placed, out_specs=rows, check_vma=False)
```

time: 332 us -> 158 us (0.48)
  Pallas kernels: 0 us -> 154 us
  waiting for transfers between devices: 139 us -> 0 us
  blocking collectives: 107 us -> 0 us
  local copies, waits for them, and re-layouts: 27.3 us -> 1.88 us
  matrix products: 22.2 us -> 0 us
  starting transfers between devices: 18.9 us -> 0 us
  other arithmetic: 16.2 us -> 1.96 us
    pallas_call x0 -> x1, Pallas kernels: none -> 154 us  [body(): pl.pallas_call(kernel, out_shape=jax.ShapeDtypeStruct(block, BF16), in_sp...]
    all_to_all x2 -> x0, waiting for transfers between devices: 139 us -> none  [the longest x1 94.8 us: body(): lax.all_to_all(expert_out, 'sp', split_axis=0, concat_axis=0, tiled=True)]
    all_to_all x1 -> x0, blocking collectives: 107 us -> none  [body(): lax.all_to_all(outgoing, 'sp', split_axis=0, concat_axis=0, tiled=True)]
    dot_general x3 -> x0, matrix products: 22.2 us -> none  [the longest x1 12.1 us: body(): jnp.dot(hidden, down_w[0], preferred_element_type=jnp.float32)]
    gather x2 -> x0, local copies, waits for them, and re-layouts: 14 us -> none  [the longest x1 7.96 us: body(): returned.reshape(experts * capacity, width)[target].astype(jnp.float32)]
    all_to_all x2 -> x0, starting transfers between devices: 12.4 us -> none  [the longest x1 7.42 us: body(): lax.all_to_all(expert_out, 'sp', split_axis=0, concat_axis=0, tiled=True)]
    reduce_sum x6 -> x0, other arithmetic: 12.3 us -> none  [the longest x1 5.47 us: body(): combined = jnp.sum(weighted.reshape(own_count, top_count, width), axis=1)]
    ppermute x2 -> x0, starting transfers between devices: 6.48 us -> none  [shifted(): return lax.ppermute(shard, axis, pairs)]
  transfers between devices with their start and end apart: 4 -> 0, of which waited for: 2 -> 0; matrix products, arithmetic and copies ran while one was open for 2% -> 0% of each run, Pallas kernels for 0% -> 0%
where the time goes in v1:
time: 158 us
  Pallas kernels  154 us (97%)
  other arithmetic  1.96 us (1%)
  local copies, waits for them, and re-layouts  1.88 us (1%)
    pallas_call x1, Pallas kernels, body(): pl.pallas_call(kernel, out_shape=jax.ShapeDtypeStruct(block, BF16), in_sp...  154 us

profile of v1, /device:TPU:1, one launch (start us, length us, event | category | flops | bytes accessed | tf_op | source)
XLA Modules:
  0.0 157.5 jit_solution(7868145059723665603)
XLA Ops:
  0.0 0.7 convert_element_type.3
  0.7 1.3 maximum_bitcast_fusion.rw_ref
  2.0 153.7 %shard_map.136 = bf16[128,2048]{1,0:T(8,128)(2,1)} custom-call(bf16[512,512]{1,0:T(8,128)(2,1)} %b_ref.1, bf16[512,512]{1,0:T(8,128)(2,1)} %c_ref.1, bf16[512,512]{1,0:T(8,128)(2,1)} %v_ref.1, f32[3,512]{1,0:T(4,128)} %taps_ref.1, bf16[512,2048]{1,0:T(8,128)(2,1)} %wproj_ref.1, bf16[128,2048]{1,0:T(8,128)(2,1)} %resid_ref.1, f32[1,2048]{1,0:T(1,128)} %bitcast.5, ...), custom_call_target="tpu_custom_call" | custom-call | tf_op jit(solution)/shard_map/pallas_call | solution.py:384
  155.6 1.9 %copy.16 = bf16[128,2048]{1,0:T(8,128)(2,1)} copy(bf16[128,2048]{1,0:T(8,128)(2,1)} %shard_map.136) | data formatting | bytes 1048576

commit v2 on v1

v2 whole, which is shorter than its diff:
```python
import jax
import jax.numpy as jnp
from jax import lax
from jax.experimental import pallas as pl
from jax.experimental.pallas import tpu as pltpu
from jax.sharding import PartitionSpec as P

EPS = 1e-06
F32 = jnp.float32
BF16 = jnp.bfloat16
MESH = pl.DeviceIdType.MESH
D = 2048
FF = 640
ROWS = 128
CAP = 16
HALF = ROWS // 2
COLS = 512
SOURCE_OF = (0, -1, 1, -2, 2, -3, 3, 4)
STEPS = ((0, 1), (1, 2), (3, 2), (5, 2), (7, 1))
MOVES = ((2, 0), (1, 0), (3, 0), (2, 1), (1, 1), (3, 1), (0, 1))


def rows_loop(count, size, fn):
    def step(i, carry):
        fn(pl.ds(pl.multiple_of(i * size, size), size))
        return carry

    lax.fori_loop(0, count, step, 0)


def kernel(
    b_hbm, c_hbm, v_hbm, wproj_hbm, resid_hbm, taps_ref, post_ref, pre_ref, moe_ref, routes_ref, weight_ref,
    gw_ref, uw_ref, dw_ref,
    out_ref,
    b_ref, c_ref, v_ref, wproj_ref, resid_ref,
    wgu, dwv, edge, prodp, mixed, pj, x2, s1, s3, ra, rb, fm, fp,
    stream, xs, rwall, pmat, wmat, sel, rin, hid, eout, rback, part, sf, ss, rf, rs,
    l_sem, w_sem, e_ss, e_rs, rw_ss, rw_rs, x_ss, x_rs, ag_ss, ag_rs, d_ss, d_rs, r_ss, r_rs, z_ss, z_rs,
):
    sp = lax.axis_index("sp")
    tp = lax.axis_index("tp")
    z = sp // 8
    k = lax.rem(sp, 8)
    y = k // 2
    c = lax.rem(k, 2)

    def zdev(by):
        return {"sp": lax.rem(z + by + 8, 8) * 8 + k, "tp": tp}

    def other_core(dc):
        return 1 - c if dc else c

    def in_plane(dy, dc):
        return lax.rem(y + dy + 4, 4) * 2 + other_core(dc)

    def pdev(index):
        return {"sp": z * 8 + index, "tp": tp}

    def xdev(by):
        return {"sp": sp, "tp": lax.rem(tp + by + 4, 4)}

    def sdev(by):
        return {"sp": lax.rem(sp + by + 64, 64), "tp": tp}

    def rcopy(src, dst, ssem, rsem, dev):
        return pltpu.make_async_remote_copy(
            src_ref=src, dst_ref=dst, send_sem=ssem, recv_sem=rsem, device_id=dev, device_id_type=MESH
        )

    barrier = pltpu.get_barrier_semaphore()
    peers = [xdev(1), xdev(-1), sdev(1), sdev(-1)]
    peers += [zdev(by) for by in range(1, 8)]
    peers += [pdev(in_plane(dy, dc)) for dy, dc in MOVES]
    for dev in peers:
        pl.semaphore_signal(barrier, inc=1, device_id=dev, device_id_type=MESH)

    pairs = ((b_hbm, b_ref), (c_hbm, c_ref), (v_hbm, v_ref), (wproj_hbm, wproj_ref), (resid_hbm, resid_ref))
    loads = [pltpu.make_async_copy(src, dst, l_sem.at[i]) for i, (src, dst) in enumerate(pairs)]
    for i in (1, 2, 0, 3, 4):
        loads[i].start()
    weights = []
    for n in range(5):
        cols = pl.ds(n * 128, 128)
        weights.append(pltpu.make_async_copy(gw_ref.at[0, :, cols], wgu.at[n, :, pl.ds(0, 128)], w_sem.at[2 * n]))
        weights.append(pltpu.make_async_copy(uw_ref.at[0, :, cols], wgu.at[n, :, pl.ds(128, 128)], w_sem.at[2 * n + 1]))
    weights.append(pltpu.make_async_copy(dw_ref.at[0], dwv, w_sem.at[10]))
    for w in weights:
        w.start()

    rwall[0, 0:4, :] = routes_ref[...].astype(F32)
    rwall[0, 4:8, :] = weight_ref[...]

    prodp[0:16, :] = jnp.zeros((16, 512), F32)
    loads[1].wait()
    loads[2].wait()
    for i in range(4):
        rows = pl.ds(i * ROWS, ROWS)
        prodp[pl.ds(16 + i * ROWS, ROWS), :] = c_ref[rows, :].astype(F32) * v_ref[rows, :].astype(F32)
    loads[0].wait()

    def mix(at, count):
        filtered = (
            prodp[at + 14 : at + 14 + count, :] * taps_ref[0:1, :]
            + prodp[at + 15 : at + 15 + count, :] * taps_ref[1:2, :]
            + prodp[at + 16 : at + 16 + count, :] * taps_ref[2:3, :]
        )
        mixed[at : at + count, :] = (b_ref[at : at + count, :].astype(F32) * filtered).astype(BF16)

    for i in range(4):
        mix(i * ROWS, ROWS)
    loads[3].wait()

    def project(t, carry):
        rows = mixed[pl.ds(pl.multiple_of(t * ROWS, ROWS), ROWS), :]
        for n in range(4):
            got = jnp.dot(rows, wproj_ref[:, n * COLS : (n + 1) * COLS], preferred_element_type=F32)
            pj[t, n // 2, :, (n % 2) * COLS : (n % 2 + 1) * COLS] = got
        return carry

    lax.fori_loop(0, 4, project, 0)
    loads[4].wait()

    pl.semaphore_wait(barrier, len(peers))

    last = pl.ds(512 - 16, 16)
    edges = [
        rcopy(c_ref.at[last], edge.at[0], e_ss.at[0], e_rs.at[0], sdev(1)),
        rcopy(v_ref.at[last], edge.at[1], e_ss.at[1], e_rs.at[1], sdev(1)),
    ]
    for e in edges:
        e.start()

    lo, hi = pl.ds(0, HALF), pl.ds(HALF, HALF)
    halves = (lo, hi)
    t1, t2, t3 = lax.rem(tp + 1, 4), lax.rem(tp + 2, 4), lax.rem(tp + 3, 4)

    def put(t, ch, h, dst, more=None):
        def step(i, carry):
            at = pl.ds(pl.multiple_of(h * HALF + i * 16, 16), 16)
            val = pj[t, ch, at, :]
            if more is not None:
                val = val + more[at, :].astype(F32)
            dst[ch, at, :] = val.astype(BF16)
            return carry

        lax.fori_loop(0, HALF // 16, step, 0)

    x_sends = {}
    for h in range(2):
        rows = halves[h]
        i = 6 * h
        x_sends["far_a", h] = rcopy(x2.at[0, rows], ra.at[rows], x_ss.at[i], x_rs.at[i], xdev(1))
        x_sends["far_b", h] = rcopy(x2.at[1, rows], rb.at[rows], x_ss.at[i + 1], x_rs.at[i + 1], xdev(-1))
        x_sends["one_b", h] = rcopy(s1.at[1, rows], fm.at[1, rows], x_ss.at[i + 2], x_rs.at[i + 2], xdev(1))
        x_sends["three_a", h] = rcopy(s3.at[0, rows], fp.at[0, rows], x_ss.at[i + 3], x_rs.at[i + 3], xdev(-1))
        x_sends["one_a", h] = rcopy(s1.at[0, rows], fm.at[0, rows], x_ss.at[i + 4], x_rs.at[i + 4], xdev(1))
        x_sends["three_b", h] = rcopy(s3.at[1, rows], fp.at[1, rows], x_ss.at[i + 5], x_rs.at[i + 5], xdev(-1))

    def x_first(h):
        put(t2, 0, h, x2)
        x_sends["far_a", h].start()
        put(t2, 1, h, x2)
        x_sends["far_b", h].start()
        put(t1, 1, h, s1)
        x_sends["one_b", h].start()
        put(t3, 0, h, s3)
        x_sends["three_a", h].start()

    def x_second(h):
        x_sends["far_a", h].wait_recv()
        put(t1, 0, h, s1, ra)
        x_sends["one_a", h].start()
        x_sends["far_b", h].wait_recv()
        put(t3, 1, h, s3, rb)
        x_sends["three_b", h].start()

    x_first(1)
    routing = [
        rcopy(rwall.at[0], rwall.at[i], rw_ss.at[i], rw_rs.at[i], zdev(-SOURCE_OF[i])) for i in range(1, 8)
    ]
    for r in routing:
        r.start()
    for e in edges:
        e.wait_recv()
    prior = edge[0].astype(F32) * edge[1].astype(F32)
    prodp[0:16, :] = jnp.where(sp > 0, prior, jnp.zeros_like(prior))
    mix(0, 16)
    for n in range(4):
        got = jnp.dot(mixed[0:16, :], wproj_ref[:, n * COLS : (n + 1) * COLS], preferred_element_type=F32)
        pj[0, n // 2, 0:16, (n % 2) * COLS : (n % 2 + 1) * COLS] = got
    x_second(1)
    x_first(0)
    x_second(0)

    for r in routing:
        r.wait_recv()

    def tables(i, carry):
        rw = rwall[i]
        row = lax.broadcasted_iota(jnp.int32, (ROWS, ROWS), 0)
        lane = lax.broadcasted_iota(jnp.int32, (ROWS, ROWS), 1)
        expert = (z * 8 + row // CAP).astype(F32)
        slot = lax.rem(row, CAP).astype(F32)
        named = jnp.zeros((ROWS, ROWS), F32)
        weight = jnp.zeros((ROWS, ROWS), F32)
        for j in range(4):
            hit = rw[j : j + 1, :] == expert
            named = named + jnp.where(hit, 1.0, 0.0)
            weight = weight + jnp.where(hit, jnp.broadcast_to(rw[4 + j : 5 + j, :], (ROWS, ROWS)), 0.0)
        before = jnp.where(row < lane, 1.0, 0.0).astype(BF16)
        earlier = jnp.dot(named.astype(BF16), before, preferred_element_type=F32)
        picked = jnp.where(earlier == slot, named, 0.0)
        pmat[i] = picked.astype(BF16)
        wt = jnp.transpose(picked * weight)
        high = wt.astype(BF16)
        wmat[i, :, 0:ROWS] = high
        wmat[i, :, ROWS : 2 * ROWS] = (wt - high.astype(F32)).astype(BF16)
        return carry

    def ag(step, half, up):
        src = (0, 1, 3, 5) if up else (0, 2, 4, 6)
        dst = (1, 3, 5, 7) if up else (2, 4, 6, 7)
        at = (0 if up else 8) + 2 * step + half
        rows = halves[half]
        return rcopy(
            xs.at[src[step], rows], xs.at[dst[step], rows], ag_ss.at[at], ag_rs.at[at], zdev(1 if up else -1)
        )

    ring = {(s, h, u): ag(s, h, u) for s in range(3) for h in range(2) for u in (True, False)}
    ring[(3, 0, True)] = ag(3, 0, True)
    ring[(3, 1, False)] = ag(3, 1, False)

    wide = (slice(0, 1024), slice(1024, 2048))

    def norms(at):
        proj = [pj[tp, n, at, :] + fm[n, at, :].astype(F32) + fp[n, at, :].astype(F32) for n in range(2)]
        square = sum(jnp.sum(p * p, axis=-1, keepdims=True) for p in proj)
        inv = lax.rsqrt(square * (1.0 / D) + EPS)
        st = [
            (resid_ref[at, wide[n]].astype(F32) + proj[n] * inv * post_ref[:, wide[n]]).astype(BF16)
            for n in range(2)
        ]
        square = jnp.zeros_like(square)
        for n in range(2):
            stream[at, wide[n]] = st[n]
            st[n] = st[n].astype(F32)
            square = square + jnp.sum(st[n] * st[n], axis=-1, keepdims=True)
        inv2 = lax.rsqrt(square * (1.0 / D) + EPS)
        for n in range(2):
            xs[0, at, wide[n]] = (st[n] * inv2 * pre_ref[:, wide[n]]).astype(BF16)

    for h in (1, 0):
        for name in ("one_b", "three_a", "one_a", "three_b"):
            x_sends[name, h].wait_recv()

        def half_rows(i, carry, h=h):
            norms(pl.ds(pl.multiple_of(h * HALF + i * 16, 16), 16))
            return carry

        lax.fori_loop(0, HALF // 16, half_rows, 0)
        ring[(0, h, True)].start()
        ring[(0, h, False)].start()
        if h == 1:
            lax.fori_loop(0, 8, tables, 0)

    def select(i):
        def cols(at):
            got = jnp.dot(pmat[i], xs[i, :, at], preferred_element_type=F32)
            sel[i, :, :, at] = got.astype(BF16).reshape(8, CAP, COLS)

        rows_loop(D // COLS, COLS, cols)

    sent, arriving = {}, {}
    for si, (first, n) in enumerate(STEPS):
        blocks = pl.ds(first, n)
        for m, (dy, dc) in enumerate(MOVES):
            to, frm = in_plane(dy, dc), in_plane(-dy, dc)
            sem, rsem = d_ss.at[si, m], d_rs.at[si, m]
            sent[si, m] = rcopy(sel.at[blocks, to], rin.at[blocks, k], sem, rsem, pdev(to))
            arriving[si, m] = rcopy(sel.at[blocks, frm], rin.at[blocks, frm], sem, rsem, pdev(to))

    def dispatch(si):
        first, n = STEPS[si]
        for i in range(first, first + n):
            select(i)
        for m in range(7):
            sent[si, m].start()
        for i in range(first, first + n):
            rin[i, k] = sel[i, k]

    def experts(si):
        first, n = STEPS[si]
        for m in range(7):
            arriving[si, m].wait_recv()
        if si == 0:
            for w in weights:
                w.wait()
        m = n * ROWS

        def gate_up(j, carry):
            x = rin[pl.ds(first, n)].reshape(m, D)
            gu = jnp.dot(x, wgu[j], preferred_element_type=F32)
            gate = jnp.minimum(gu[:, 0:128], 7.0)
            up = jnp.clip(gu[:, 128:256], -7.0, 7.0)
            hid[j, 0:m, :] = (gate * jax.nn.sigmoid(1.702 * gate) * (up + 1.0)).astype(BF16)
            return carry

        lax.fori_loop(0, 5, gate_up, 0)

        def down(at):
            h = jnp.concatenate([hid[j, 0:m, :] for j in range(5)], axis=1)
            got = jnp.dot(h, dwv[:, at], preferred_element_type=F32)
            eout[pl.ds(first, n), :, :, at] = got.astype(BF16).reshape(n, 8, CAP, COLS)

        rows_loop(D // COLS, COLS, down)
        for i in range(first, first + n):
            rback[i, k] = eout[i, k]

    def block_of(slot, core):
        if slot == 0:
            return 7
        if slot == 7:
            return 0
        base = (5, 3, 1)[(slot - 1) // 2]
        return base + 1 - core if slot % 2 else base + core

    returned, coming = {}, {}
    for slot in range(8):
        for m, (dy, dc) in enumerate(MOVES):
            to, frm = in_plane(dy, dc), in_plane(-dy, dc)
            sem, rsem = r_ss.at[slot, m], r_rs.at[slot, m]
            theirs, mine = block_of(slot, other_core(dc)), block_of(slot, c)
            returned[slot, m] = rcopy(eout.at[theirs, to], rback.at[theirs, k], sem, rsem, pdev(to))
            coming[slot, m] = rcopy(eout.at[mine, frm], rback.at[mine, frm], sem, rsem, pdev(to))

    def send_back(slot):
        for m in range(7):
            returned[slot, m].start()

    dispatch(0)
    for s in range(1, 4):
        for h in (1, 0):
            for u in (True, False):
                ring[(s - 1, h, u)].wait_recv()
                if (s, h, u) in ring:
                    ring[(s, h, u)].start()
            if h == 1 and s >= 2:
                experts(s - 2)
        dispatch(s)
    experts(2)
    ring[(3, 0, True)].wait_recv()
    ring[(3, 1, False)].wait_recv()
    dispatch(4)
    send_back(7)
    experts(3)
    experts(4)
    for slot in range(7):
        send_back(slot)

    def combine(i, ch, dst, more=None):
        for n in range(2):
            at = slice(ch * 1024 + n * COLS, ch * 1024 + (n + 1) * COLS)
            here = slice(n * COLS, (n + 1) * COLS)
            r = rback[i, :, :, at].reshape(ROWS, COLS)
            got = jnp.dot(wmat[i, :, 0:ROWS], r, preferred_element_type=F32)
            got = got + jnp.dot(wmat[i, :, ROWS : 2 * ROWS], r, preferred_element_type=F32)
            if more is not None:
                got = got + more[:, here].astype(F32)
            dst[:, here] = got.astype(dst.dtype)

    def zsend(r, ch, f):
        at = (0 if f else 8) + 2 * r + ch
        src, dst = (sf, rf) if f else (ss, rs)
        return rcopy(src.at[r, ch], dst.at[r, ch], z_ss.at[at], z_rs.at[at], zdev(1 - 2 * c if f else 2 * c - 1))

    chain = {(r, ch, f): zsend(r, ch, f) for r in range(1, 4) for ch in range(2) for f in (True, False)}
    chain[(0, 0, True)] = zsend(0, 0, True)
    chain[(0, 1, False)] = zsend(0, 1, False)

    def take(slot):
        for m in range(7):
            coming[slot, m].wait_recv()

    take(7)
    combine(0, 0, part.at[0])
    combine(0, 1, part.at[1])
    take(0)
    combine(7, 0, sf.at[0, 0])
    chain[(0, 0, True)].start()
    combine(7, 1, ss.at[0, 1])
    chain[(0, 1, False)].start()
    for slot in range(1, 7):
        r, f = (slot + 1) // 2, slot % 2 == 1
        send, got = (sf, rf) if f else (ss, rs)
        take(slot)
        i = block_of(slot, c)
        for ch in ((1, 0) if f else (0, 1)):
            if (r - 1, ch, f) in chain:
                chain[(r - 1, ch, f)].wait_recv()
                combine(i, ch, send.at[r, ch], got.at[r - 1, ch])
            else:
                combine(i, ch, send.at[r, ch])
            chain[(r, ch, f)].start()

    for f, ch in ((True, 1), (True, 0), (False, 0), (False, 1)):
        chain[(3, ch, f)].wait_recv()

    def finish(at):
        total = [part[n, at, :] + rf[3, n, at, :].astype(F32) + rs[3, n, at, :].astype(F32) for n in range(2)]
        square = sum(jnp.sum(t * t, axis=-1, keepdims=True) for t in total)
        inv = lax.rsqrt(square * (1.0 / D) + EPS)
        for n in range(2):
            gained = total[n] * inv * moe_ref[:, wide[n]]
            out_ref[at, wide[n]] = (stream[at, wide[n]].astype(F32) + gained).astype(BF16)

    rows_loop(ROWS // 16, 16, finish)

    for group in (edges, routing, x_sends.values(), ring.values(), chain.values(), sent.values(), returned.values()):
        for s in group:
            s.wait_send()


def body(
    b_gate, c_gate, values_in, conv_taps, out_proj, resid, post_gain, pre_gain, moe_gain,
    routes, route_weight, gate_w, up_w, down_w,
):
    vmem = pl.BlockSpec(memory_space=pltpu.VMEM)
    hbm = pl.BlockSpec(memory_space=pl.ANY)
    dma = pltpu.SemaphoreType.DMA
    block = (ROWS, D)
    split = (2, ROWS, D // 2)
    return pl.pallas_call(
        kernel,
        out_shape=jax.ShapeDtypeStruct(block, BF16),
        in_specs=[hbm] * 5 + [vmem] * 6 + [hbm] * 3,
        out_specs=vmem,
        scratch_shapes=[
            pltpu.VMEM((512, 512), BF16),
            pltpu.VMEM((512, 512), BF16),
            pltpu.VMEM((512, 512), BF16),
            pltpu.VMEM((512, D), BF16),
            pltpu.VMEM(block, BF16),
            pltpu.VMEM((5, D, 256), BF16),
            pltpu.VMEM((FF, D), BF16),
            pltpu.VMEM((2, 16, 512), BF16),
            pltpu.VMEM((528, 512), F32),
            pltpu.VMEM((512, 512), BF16),
            pltpu.VMEM((4,) + split, F32),
            pltpu.VMEM(split, BF16),
            pltpu.VMEM(split, BF16),
            pltpu.VMEM(split, BF16),
            pltpu.VMEM((ROWS, D // 2), BF16),
            pltpu.VMEM((ROWS, D // 2), BF16),
            pltpu.VMEM(split, BF16),
            pltpu.VMEM(split, BF16),
            pltpu.VMEM(block, BF16),
            pltpu.VMEM((8,) + block, BF16),
            pltpu.VMEM((8, 8, 128), F32),
            pltpu.VMEM((8, ROWS, ROWS), BF16),
            pltpu.VMEM((8, ROWS, 2 * ROWS), BF16),
            pltpu.VMEM((8, 8, CAP, D), BF16),
            pltpu.VMEM((8, 8, CAP, D), BF16),
            pltpu.VMEM((5, 2 * ROWS, 128), BF16),
            pltpu.VMEM((8, 8, CAP, D), BF16),
            pltpu.VMEM((8, 8, CAP, D), BF16),
            pltpu.VMEM(split, F32),
            pltpu.VMEM((4,) + split, BF16),
            pltpu.VMEM((4,) + split, BF16),
            pltpu.VMEM((4,) + split, BF16),
            pltpu.VMEM((4,) + split, BF16),
            dma((5,)), dma((11,)),
            dma((2,)), dma((2,)),
            dma((8,)), dma((8,)),
            dma((12,)), dma((12,)),
            dma((16,)), dma((16,)),
            dma((5, 7)), dma((5, 7)),
            dma((8, 7)), dma((8, 7)),
            dma((16,)), dma((16,)),
        ],
        compiler_params=pltpu.CompilerParams(
            collective_id=0, has_side_effects=True, vmem_limit_bytes=63 * 2**20
        ),
    )(
        b_gate, c_gate, values_in, out_proj, resid, conv_taps,
        post_gain.reshape(1, D), pre_gain.reshape(1, D), moe_gain.reshape(1, D), routes.T, route_weight.T,
        gate_w, up_w, down_w,
    )


def solution(mesh):
    rows = P(("sp", "tp"), None)
    placed = (
        P("sp", "tp"), P("sp", "tp"), P("sp", "tp"), P(None, "tp"), P("tp", None), rows,
        P(), P(), P(), rows, rows,
        P("sp", None, None), P("sp", None, None), P("sp", None, None),
    )
    return jax.shard_map(body, mesh=mesh, in_specs=placed, out_specs=rows, check_vma=False)
```

time: 158 us -> 145 us (0.918)
  Pallas kernels: 154 us -> 143 us
  other arithmetic: 1.96 us -> 0 us
    pallas_call x1, Pallas kernels: 154 us -> 143 us  [body(): pl.pallas_call(kernel, out_shape=jax.ShapeDtypeStruct(block, BF16), in_sp...]
where the time goes in v2:
time: 145 us
  Pallas kernels  143 us (99%)
  local copies, waits for them, and re-layouts  1.88 us (1%)
    pallas_call x1, Pallas kernels, body(): pl.pallas_call(kernel, out_shape=jax.ShapeDtypeStruct(block, BF16), in_sp...  143 us

profile of v2, /device:TPU:1, one launch (start us, length us, event | category | flops | bytes accessed | tf_op | source)
XLA Modules:
  0.0 144.9 jit_solution(7228508186575963871)
XLA Ops:
  0.0 143.0 %shard_map.136 = bf16[128,2048]{1,0:T(8,128)(2,1)} custom-call(bf16[512,512]{1,0:T(8,128)(2,1)} %b_hbm.1, bf16[512,512]{1,0:T(8,128)(2,1)} %c_hbm.1, bf16[512,512]{1,0:T(8,128)(2,1)} %v_hbm.1, bf16[512,2048]{1,0:T(8,128)(2,1)} %wproj_hbm.1, bf16[128,2048]{1,0:T(8,128)(2,1)} %resid_hbm.1, f32[3,512]{1,0:T(4,128)} %taps_ref.1, f32[1,2048]{1,0:T(1,128)} %bitcast.5, ...), custom_call_target="tpu_custom_call" | custom-call | tf_op jit(solution)/shard_map/pallas_call | solution.py:432
  143.0 1.9 %copy.16 = bf16[128,2048]{1,0:T(8,128)(2,1)} copy(bf16[128,2048]{1,0:T(8,128)(2,1)} %shard_map.136) | data formatting | bytes 1048576

commit v3 on v2

--- a/solution.py
+++ b/solution.py
@@ -15,8 +15,7 @@
 CAP = 16
 HALF = ROWS // 2
 COLS = 512
-SOURCE_OF = (0, -1, 1, -2, 2, -3, 3, 4)
-STEPS = ((0, 1), (1, 2), (3, 2), (5, 2), (7, 1))
+PARTED = (7, 1, 2, 3, 4, 5, 6)
 MOVES = ((2, 0), (1, 0), (3, 0), (2, 1), (1, 1), (3, 1), (0, 1))
 
 
@@ -43,6 +42,7 @@
     k = lax.rem(sp, 8)
     y = k // 2
     c = lax.rem(k, 2)
+    turn = 1 - 2 * c
 
     def zdev(by):
         return {"sp": lax.rem(z + by + 8, 8) * 8 + k, "tp": tp}
@@ -156,11 +156,13 @@
         x_sends["one_a", h] = rcopy(s1.at[0, rows], fm.at[0, rows], x_ss.at[i + 4], x_rs.at[i + 4], xdev(1))
         x_sends["three_b", h] = rcopy(s3.at[1, rows], fp.at[1, rows], x_ss.at[i + 5], x_rs.at[i + 5], xdev(-1))
 
-    def x_first(h):
+    def x_far(h):
         put(t2, 0, h, x2)
         x_sends["far_a", h].start()
         put(t2, 1, h, x2)
         x_sends["far_b", h].start()
+
+    def x_near(h):
         put(t1, 1, h, s1)
         x_sends["one_b", h].start()
         put(t3, 0, h, s3)
@@ -174,9 +176,11 @@
         put(t3, 1, h, s3, rb)
         x_sends["three_b", h].start()
 
-    x_first(1)
+    x_far(1)
+    x_near(1)
     routing = [
-        rcopy(rwall.at[0], rwall.at[i], rw_ss.at[i], rw_rs.at[i], zdev(-SOURCE_OF[i])) for i in range(1, 8)
+        rcopy(rwall.at[0], rwall.at[i], rw_ss.at[i], rw_rs.at[i], zdev(turn * ((i + 1) // 2) * (1 if i % 2 else -1)))
+        for i in range(1, 8)
     ]
     for r in routing:
         r.start()
@@ -188,9 +192,9 @@
     for n in range(4):
         got = jnp.dot(mixed[0:16, :], wproj_ref[:, n * COLS : (n + 1) * COLS], preferred_element_type=F32)
         pj[0, n // 2, 0:16, (n % 2) * COLS : (n % 2 + 1) * COLS] = got
+    x_far(0)
     x_second(1)
-    x_first(0)
-    x_second(0)
+    x_near(0)
 
     for r in routing:
         r.wait_recv()
@@ -217,18 +221,24 @@
         wmat[i, :, ROWS : 2 * ROWS] = (wt - high.astype(F32)).astype(BF16)
         return carry
 
-    def ag(step, half, up):
-        src = (0, 1, 3, 5) if up else (0, 2, 4, 6)
-        dst = (1, 3, 5, 7) if up else (2, 4, 6, 7)
-        at = (0 if up else 8) + 2 * step + half
+    lax.fori_loop(0, 8, tables, 0)
+    x_second(0)
+
+    def ag(step, half, f):
+        src = 0 if step == 0 else 2 * step - 1 if f else 2 * step
+        dst = min(2 * step + 1 if f else 2 * step + 2, 7)
+        at = (0 if f else 8) + 2 * step + half
         rows = halves[half]
-        return rcopy(
-            xs.at[src[step], rows], xs.at[dst[step], rows], ag_ss.at[at], ag_rs.at[at], zdev(1 if up else -1)
-        )
-
-    ring = {(s, h, u): ag(s, h, u) for s in range(3) for h in range(2) for u in (True, False)}
-    ring[(3, 0, True)] = ag(3, 0, True)
-    ring[(3, 1, False)] = ag(3, 1, False)
+        return rcopy(xs.at[src, rows], xs.at[dst, rows], ag_ss.at[at], ag_rs.at[at], zdev(turn if f else -turn))
+
+    ring = {(s, h, f): ag(s, h, f) for s in range(3) for h in range(2) for f in (True, False)}
+    ring[(3, 1, True)] = ag(3, 1, True)
+    ring[(3, 0, False)] = ag(3, 0, False)
+
+    def forward(step, half, f):
+        ring[(step - 1, half, f)].wait_recv()
+        if (step, half, f) in ring:
+            ring[(step, half, f)].start()
 
     wide = (slice(0, 1024), slice(1024, 2048))
 
@@ -249,19 +259,15 @@
         for n in range(2):
             xs[0, at, wide[n]] = (st[n] * inv2 * pre_ref[:, wide[n]]).astype(BF16)
 
-    for h in (1, 0):
+    def normed_rows(h):
         for name in ("one_b", "three_a", "one_a", "three_b"):
             x_sends[name, h].wait_recv()
 
-        def half_rows(i, carry, h=h):
+        def half_rows(i, carry):
             norms(pl.ds(pl.multiple_of(h * HALF + i * 16, 16), 16))
             return carry
 
         lax.fori_loop(0, HALF // 16, half_rows, 0)
-        ring[(0, h, True)].start()
-        ring[(0, h, False)].start()
-        if h == 1:
-            lax.fori_loop(0, 8, tables, 0)
 
     def select(i):
         def cols(at):
@@ -270,29 +276,36 @@
 
         rows_loop(D // COLS, COLS, cols)
 
-    sent, arriving = {}, {}
-    for si, (first, n) in enumerate(STEPS):
-        blocks = pl.ds(first, n)
+    sent, arriving, returned, coming = {}, {}, {}, {}
+    for slot in range(8):
         for m, (dy, dc) in enumerate(MOVES):
             to, frm = in_plane(dy, dc), in_plane(-dy, dc)
-            sem, rsem = d_ss.at[si, m], d_rs.at[si, m]
-            sent[si, m] = rcopy(sel.at[blocks, to], rin.at[blocks, k], sem, rsem, pdev(to))
-            arriving[si, m] = rcopy(sel.at[blocks, frm], rin.at[blocks, frm], sem, rsem, pdev(to))
-
-    def dispatch(si):
-        first, n = STEPS[si]
+            sems = d_ss.at[slot, m], d_rs.at[slot, m]
+            sent[slot, m] = rcopy(sel.at[slot, to], rin.at[slot, k], *sems, pdev(to))
+            arriving[slot, m] = rcopy(sel.at[slot, frm], rin.at[slot, frm], *sems, pdev(to))
+            for ch in (0, 1) if slot in PARTED else (0,):
+                cols = pl.ds(1024 * ch, 1024 if slot in PARTED else D)
+                sems = r_ss.at[slot + 8 * ch, m], r_rs.at[slot + 8 * ch, m]
+                returned[slot, ch, m] = rcopy(eout.at[slot, to, :, cols], rback.at[slot, k, :, cols], *sems, pdev(to))
+                coming[slot, ch, m] = rcopy(eout.at[slot, frm, :, cols], rback.at[slot, frm, :, cols], *sems, pdev(to))
+
+    def dispatch(slot):
+        for m in range(7):
+            sent[slot, m].start()
+        rin[slot, k] = sel[slot, k]
+
+    def send_back(slot, ch=0):
+        for m in range(7):
+            returned[slot, ch, m].start()
+
+    def order_of(slot):
+        return (1, 0) if slot % 2 == 1 else (0, 1)
+
+    def experts(first, n, parted=False):
         for i in range(first, first + n):
-            select(i)
-        for m in range(7):
-            sent[si, m].start()
-        for i in range(first, first + n):
-            rin[i, k] = sel[i, k]
-
-    def experts(si):
-        first, n = STEPS[si]
-        for m in range(7):
-            arriving[si, m].wait_recv()
-        if si == 0:
+            for m in range(7):
+                arriving[i, m].wait_recv()
+        if first == 0:
             for w in weights:
                 w.wait()
         m = n * ROWS
@@ -312,50 +325,63 @@
             got = jnp.dot(h, dwv[:, at], preferred_element_type=F32)
             eout[pl.ds(first, n), :, :, at] = got.astype(BF16).reshape(n, 8, CAP, COLS)
 
-        rows_loop(D // COLS, COLS, down)
+        if parted:
+            for half in range(2):
+                for n_ in range(2):
+                    down(pl.ds(half * 1024 + n_ * COLS, COLS))
+                send_back(7, half)
+        else:
+            rows_loop(D // COLS, COLS, down)
         for i in range(first, first + n):
             rback[i, k] = eout[i, k]
 
-    def block_of(slot, core):
-        if slot == 0:
-            return 7
-        if slot == 7:
-            return 0
-        base = (5, 3, 1)[(slot - 1) // 2]
-        return base + 1 - core if slot % 2 else base + core
-
-    returned, coming = {}, {}
-    for slot in range(8):
-        for m, (dy, dc) in enumerate(MOVES):
-            to, frm = in_plane(dy, dc), in_plane(-dy, dc)
-            sem, rsem = r_ss.at[slot, m], r_rs.at[slot, m]
-            theirs, mine = block_of(slot, other_core(dc)), block_of(slot, c)
-            returned[slot, m] = rcopy(eout.at[theirs, to], rback.at[theirs, k], sem, rsem, pdev(to))
-            coming[slot, m] = rcopy(eout.at[mine, frm], rback.at[mine, frm], sem, rsem, pdev(to))
-
-    def send_back(slot):
-        for m in range(7):
-            returned[slot, m].start()
-
+    normed_rows(1)
+    ring[(0, 1, True)].start()
+    ring[(0, 1, False)].start()
+    normed_rows(0)
+    ring[(0, 0, True)].start()
+    select(0)
     dispatch(0)
-    for s in range(1, 4):
-        for h in (1, 0):
-            for u in (True, False):
-                ring[(s - 1, h, u)].wait_recv()
-                if (s, h, u) in ring:
-                    ring[(s, h, u)].start()
-            if h == 1 and s >= 2:
-                experts(s - 2)
-        dispatch(s)
-    experts(2)
-    ring[(3, 0, True)].wait_recv()
-    ring[(3, 1, False)].wait_recv()
+    ring[(0, 0, False)].start()
+    forward(1, 1, True)
+    forward(1, 1, False)
+    forward(1, 0, True)
+    select(1)
+    dispatch(1)
+    forward(1, 0, False)
+    select(2)
+    dispatch(2)
+    experts(0, 1)
+    forward(2, 1, True)
+    forward(2, 0, True)
+    select(3)
+    dispatch(3)
+    forward(2, 1, False)
+    forward(2, 0, False)
+    select(4)
     dispatch(4)
-    send_back(7)
-    experts(3)
-    experts(4)
-    for slot in range(7):
-        send_back(slot)
+    experts(1, 2)
+    forward(3, 1, True)
+    forward(3, 0, True)
+    select(5)
+    dispatch(5)
+    forward(3, 0, False)
+    forward(3, 1, False)
+    select(6)
+    ring[(3, 1, True)].wait_recv()
+    ring[(3, 0, False)].wait_recv()
+    select(7)
+    dispatch(7)
+    dispatch(6)
+    experts(3, 2)
+    experts(5, 1)
+    experts(7, 1, True)
+    for ch in order_of(5) if 5 in PARTED else (0,):
+        send_back(5, ch)
+    experts(6, 1)
+    for slot in (6, 3, 4, 1, 2, 0):
+        for ch in order_of(slot) if slot in PARTED else (0,):
+            send_back(slot, ch)
 
     def combine(i, ch, dst, more=None):
         for n in range(2):
@@ -371,37 +397,41 @@
     def zsend(r, ch, f):
         at = (0 if f else 8) + 2 * r + ch
         src, dst = (sf, rf) if f else (ss, rs)
-        return rcopy(src.at[r, ch], dst.at[r, ch], z_ss.at[at], z_rs.at[at], zdev(1 - 2 * c if f else 2 * c - 1))
+        return rcopy(src.at[r, ch], dst.at[r, ch], z_ss.at[at], z_rs.at[at], zdev(-turn if f else turn))
 
     chain = {(r, ch, f): zsend(r, ch, f) for r in range(1, 4) for ch in range(2) for f in (True, False)}
     chain[(0, 0, True)] = zsend(0, 0, True)
     chain[(0, 1, False)] = zsend(0, 1, False)
 
-    def take(slot):
+    def take(slot, ch=0):
         for m in range(7):
-            coming[slot, m].wait_recv()
+            coming[slot, ch, m].wait_recv()
 
     take(7)
+    combine(7, 0, sf.at[0, 0])
+    chain[(0, 0, True)].start()
+    take(7, 1)
+    combine(7, 1, ss.at[0, 1])
+    chain[(0, 1, False)].start()
+    for slot in (5, 6, 3, 4, 1, 2):
+        f = slot % 2 == 1
+        r = 4 - (slot + 1) // 2
+        send, got = (sf, rf) if f else (ss, rs)
+        if slot not in PARTED:
+            take(slot)
+        for ch in order_of(slot):
+            if slot in PARTED:
+                take(slot, ch)
+            if (r - 1, ch, f) in chain:
+                chain[(r - 1, ch, f)].wait_recv()
+                combine(slot, ch, send.at[r, ch], got.at[r - 1, ch])
+            else:
+                combine(slot, ch, send.at[r, ch])
+            chain[(r, ch, f)].start()
+
+    take(0)
     combine(0, 0, part.at[0])
     combine(0, 1, part.at[1])
-    take(0)
-    combine(7, 0, sf.at[0, 0])
-    chain[(0, 0, True)].start()
-    combine(7, 1, ss.at[0, 1])
-    chain[(0, 1, False)].start()
-    for slot in range(1, 7):
-        r, f = (slot + 1) // 2, slot % 2 == 1
-        send, got = (sf, rf) if f else (ss, rs)
-        take(slot)
-        i = block_of(slot, c)
-        for ch in ((1, 0) if f else (0, 1)):
-            if (r - 1, ch, f) in chain:
-                chain[(r - 1, ch, f)].wait_recv()
-                combine(i, ch, send.at[r, ch], got.at[r - 1, ch])
-            else:
-                combine(i, ch, send.at[r, ch])
-            chain[(r, ch, f)].start()
-
     for f, ch in ((True, 1), (True, 0), (False, 0), (False, 1)):
         chain[(3, ch, f)].wait_recv()
 
@@ -415,7 +445,8 @@
 
     rows_loop(ROWS // 16, 16, finish)
 
-    for group in (edges, routing, x_sends.values(), ring.values(), chain.values(), sent.values(), returned.values()):
+    late = [ring[key] for key in ring]
+    for group in (edges, routing, x_sends.values(), late, chain.values(), sent.values(), returned.values()):
         for s in group:
             s.wait_send()
 
@@ -473,8 +504,8 @@
             dma((8,)), dma((8,)),
             dma((12,)), dma((12,)),
             dma((16,)), dma((16,)),
-            dma((5, 7)), dma((5, 7)),
             dma((8, 7)), dma((8, 7)),
+            dma((16, 7)), dma((16, 7)),
             dma((16,)), dma((16,)),
         ],
         compiler_params=pltpu.CompilerParams(

time: 145 us -> 138 us (0.952)
  Pallas kernels: 143 us -> 136 us
    pallas_call x1, Pallas kernels: 143 us -> 136 us  [body(): pl.pallas_call(kernel, out_shape=jax.ShapeDtypeStruct(block, BF16), in_sp...]
where the time goes in v3:
time: 138 us
  Pallas kernels  136 us (99%)
  local copies, waits for them, and re-layouts  1.88 us (1%)
    pallas_call x1, Pallas kernels, body(): pl.pallas_call(kernel, out_shape=jax.ShapeDtypeStruct(block, BF16), in_sp...  136 us

profile of v3, /device:TPU:1, one launch (start us, length us, event | category | flops | bytes accessed | tf_op | source)
XLA Modules:
  0.0 137.7 jit_solution(11062145613149217749)
XLA Ops:
  0.0 135.8 %shard_map.136 = bf16[128,2048]{1,0:T(8,128)(2,1)} custom-call(bf16[512,512]{1,0:T(8,128)(2,1)} %b_hbm.1, bf16[512,512]{1,0:T(8,128)(2,1)} %c_hbm.1, bf16[512,512]{1,0:T(8,128)(2,1)} %v_hbm.1, bf16[512,2048]{1,0:T(8,128)(2,1)} %wproj_hbm.1, bf16[128,2048]{1,0:T(8,128)(2,1)} %resid_hbm.1, f32[3,512]{1,0:T(4,128)} %taps_ref.1, f32[1,2048]{1,0:T(1,128)} %bitcast.5, ...), custom_call_target="tpu_custom_call" | custom-call | tf_op jit(solution)/shard_map/pallas_call | solution.py:463
  135.9 1.9 %copy.16 = bf16[128,2048]{1,0:T(8,128)(2,1)} copy(bf16[128,2048]{1,0:T(8,128)(2,1)} %shard_map.136) | data formatting | bytes 1048576

commit v4 on v3

--- a/solution.py
+++ b/solution.py
@@ -340,9 +340,9 @@
     ring[(0, 1, False)].start()
     normed_rows(0)
     ring[(0, 0, True)].start()
+    ring[(0, 0, False)].start()
     select(0)
     dispatch(0)
-    ring[(0, 0, False)].start()
     forward(1, 1, True)
     forward(1, 1, False)
     forward(1, 0, True)

time: 138 us -> 138 us (level)
  no operation moved by 1% of the time
where the time goes in v4:
time: 138 us; the launch traced here: 137 us
  Pallas kernels  136 us (99%)
  local copies, waits for them, and re-layouts  1.88 us (1%)
    pallas_call x1, Pallas kernels, body(): pl.pallas_call(kernel, out_shape=jax.ShapeDtypeStruct(block, BF16), in_sp...  136 us

profile of v4, /device:TPU:1, one launch (start us, length us, event | category | flops | bytes accessed | tf_op | source)
XLA Modules:
  0.0 137.4 jit_solution(4547023036934726007)
XLA Ops:
  0.0 135.5 %shard_map.136 = bf16[128,2048]{1,0:T(8,128)(2,1)} custom-call(bf16[512,512]{1,0:T(8,128)(2,1)} %b_hbm.1, bf16[512,512]{1,0:T(8,128)(2,1)} %c_hbm.1, bf16[512,512]{1,0:T(8,128)(2,1)} %v_hbm.1, bf16[512,2048]{1,0:T(8,128)(2,1)} %wproj_hbm.1, bf16[128,2048]{1,0:T(8,128)(2,1)} %resid_hbm.1, f32[3,512]{1,0:T(4,128)} %taps_ref.1, f32[1,2048]{1,0:T(1,128)} %bitcast.5, ...), custom_call_target="tpu_custom_call" | custom-call | tf_op jit(solution)/shard_map/pallas_call | solution.py:463
  135.5 1.9 %copy.16 = bf16[128,2048]{1,0:T(8,128)(2,1)} copy(bf16[128,2048]{1,0:T(8,128)(2,1)} %shard_map.136) | data formatting | bytes 1048576
